TPU v7x, 32 devices: a whole 2x2x4 slice. The times are simulated.
32 devices in a mesh: grp: 2 (over x), tp: 4 (over y, core), dp: 4 (over z).
Axes of the slice: x: 2, y: 2, z: 4, core: 2. Of those that a mesh axis runs over, the one named last changes fastest.
Arguments:
- tokens: bfloat16 [512, 2048], P(('grp', 'tp'), 'dp'), parts along dimension 0, may hold values from -25 to 25
- state: float32 [2, 512, 16, 128, 128], P(None, ('grp', 'dp'), 'tp'), parts along dimension 1, may hold values from -1 to 1
- lengths: int32 [512], P(('grp', 'dp')), parts along dimension 0, may hold values from 1 to 4096, 131072 in all
- norm_gain: bfloat16 [2, 2048], P(None, 'dp'), may hold values from 0.099609375 to 1.8984375
- w_query: bfloat16 [2, 2048, 2048], P(None, 'dp', 'tp'), may hold values from -0.125 to 0.125
- w_forget: bfloat16 [2, 2048, 2048], P(None, 'dp', 'tp'), may hold values from -0.125 to 0.125
- w_input: bfloat16 [2, 2048, 2048], P(None, 'dp', 'tp'), may hold values from -0.125 to 0.125
- w_gate: bfloat16 [2, 2048, 2048], P(None, 'dp', 'tp'), may hold values from -0.125 to 0.125
- w_out: bfloat16 [2, 2048, 2048], P(None, 'tp', 'dp'), may hold values from -0.125 to 0.125
- bound_logit: float32 [2, 2048], P(None, 'tp'), may hold values from -3 to 5
- pace: float32 [2, 2048], P(None, 'tp'), may hold values from 0.6 to 2
- head_gain: float32 [2, 128], replicated, may hold values from 0.4 to 2.5
Outputs:
- mixed: float32 [512, 2048], P(('grp', 'tp'), 'dp'), parts along dimension 0
- new_state: float32 [2, 512, 16, 128, 128], P(None, ('grp', 'dp'), 'tp'), parts along dimension 1
There are 2 independent parts, one for each index of `grp`. A program takes and returns all parts, laid end to end along the dimension named above; an argument that names none is the same for every part. Nothing has to cross between parts.
All inputs are finite; a program needn't handle non-finite values. No bound on the sum of `lengths` on one device may be relied on, other than what follows from the above.
Results may differ from a plain program's by a relative error of at most 0.0083.
Values may be sent and summed in bfloat16 or wider, within the bound.
A program may use at most 192 MiB of HBM per device.

v0:
```python
import jax
import jax.numpy as jnp
from jax import lax
from jax.sharding import PartitionSpec as P

D = 2048
LENGTH_MEAN = 512
epsilon = 1e-06


def advance(prior, query, forget_in, value, gate, lower, pace_row, log_len, gain_row):
    count, width = query.shape
    size = prior.shape[-1]
    heads = width // size
    pre = forget_in - pace_row[None, :] * log_len[:, None]
    forget = lower[None, :] + (1.0 - lower[None, :]) * jax.nn.sigmoid(pre)
    key = (1.0 - lower[None, :]) * jax.nn.sigmoid(-pre)
    forget = forget.reshape(count, heads, size)
    key = key.reshape(count, heads, size)
    values = value.reshape(count, heads, size)
    updated = forget[..., None] * prior + key[..., None] * values[:, :, None, :]
    readout = jnp.einsum(
        "bhk,bhkv->bhv", query.reshape(count, heads, size), updated, precision=lax.Precision.HIGHEST
    )
    normed = readout * lax.rsqrt(jnp.mean(readout * readout, axis=-1, keepdims=True) + epsilon)
    gates = gate.reshape(count, heads, size)
    normed = normed * gain_row[None, None, :] * jax.nn.silu(gates)
    return (updated, normed.reshape(count, width).astype(jnp.bfloat16))


def shards(
    tokens,
    state,
    lengths,
    norm_gain,
    w_query,
    w_forget,
    w_input,
    w_gate,
    w_out,
    bound_logit,
    pace,
    head_gain,
):
    current = tokens
    log_len = jnp.log(lengths.astype(jnp.float32) / LENGTH_MEAN)
    own_count = state.shape[1]
    states = []
    result = None
    for block in range(2):
        whole = lax.all_gather(current, "tp", axis=0, tiled=True)
        whole_wide = whole.astype(jnp.float32)
        partial_sq = jnp.sum(whole_wide * whole_wide, axis=1)
        squares_all = lax.psum(partial_sq, "dp")
        squares = lax.dynamic_slice_in_dim(
            squares_all, lax.axis_index("dp") * own_count, own_count, 0
        )
        gained = (whole_wide * norm_gain[block].astype(jnp.float32)[None, :]).astype(jnp.bfloat16)
        terms = tuple(
            (
                jnp.dot(gained, weight[block], preferred_element_type=jnp.float32)
                for weight in (w_query, w_forget, w_input, w_gate)
            )
        )
        sums = lax.psum_scatter(terms, "dp", scatter_dimension=0, tiled=True)
        scale = lax.rsqrt(squares / D + epsilon)
        made = [scale[:, None] * total for total in sums]
        lower = jax.nn.sigmoid(bound_logit[block])
        updated, normed = advance(
            state[block],
            made[0],
            made[1],
            made[2],
            made[3],
            lower,
            pace[block],
            log_len,
            head_gain[block],
        )
        states.append(updated)
        gathered = lax.all_gather(normed, "dp", axis=0, tiled=True)
        out_weight = w_out[block]
        branch = lax.psum_scatter(
            jnp.dot(gathered, out_weight, preferred_element_type=jnp.float32),
            "tp",
            scatter_dimension=0,
            tiled=True,
        )
        if block == 0:
            current = (current.astype(jnp.float32) + branch).astype(jnp.bfloat16)
        else:
            result = current.astype(jnp.float32) + branch
    return (result, jnp.stack(states))


def solution(mesh):
    in_specs = (
        P(("grp", "tp"), "dp"),
        P(None, ("grp", "dp"), "tp", None, None),
        P(("grp", "dp")),
        P(None, "dp"),
        P(None, "dp", "tp"),
        P(None, "dp", "tp"),
        P(None, "dp", "tp"),
        P(None, "dp", "tp"),
        P(None, "tp", "dp"),
        P(None, "tp"),
        P(None, "tp"),
        P(),
    )
    out_specs = (P(("grp", "tp"), "dp"), P(None, ("grp", "dp"), "tp", None, None))
    return jax.shard_map(shards, mesh=mesh, in_specs=in_specs, out_specs=out_specs, check_vma=False)
```

profile of v0, /device:TPU:0, one launch (start us, length us, event | category | flops | bytes accessed | tf_op | source)
XLA Modules:
  0.0 361.6 jit_solution(16375477499638168452)
XLA Ops:
  7.2 0.8 slice_convert_fusion
  8.0 7.4 %all_gather.12 = bf16[256,512]{1,0:T(8,128)(2,1)S(1)} all-gather(bf16[64,512]{1,0:T(8,128)(2,1)} %param.12), channel_id=1, replica_groups=mesh['grp'=2,'tp'=4,'dp'=4] {'tp'}, dimensions={0}, use_global_device_ids=true | all-gather | bytes 327680 | tf_op jit(solution)/shard_map/all_gather | solution.py:51
  15.4 2.1 fusion.36
  17.6 2.1 fusion.34
  19.8 2.2 fusion.32
  22.1 2.2 fusion.38
  24.3 0.1 fusion.16
  24.5 12.0 %psum.14 = f32[256]{0:T(256)S(1)} all-reduce(f32[256]{0:T(256)S(1)} %fusion.16), channel_id=1, replica_groups=mesh['grp'=2,'tp'=4,'dp'=4] {'dp'}, use_global_device_ids=true, to_apply=%region_1.0 | all-reduce | flops 256 | bytes 2048 | tf_op jit(solution)/shard_map/psum | solution.py:54
  36.4 0.1 add_rsqrt_fusion.3
  36.5 0.7 multiply_log_fusion
  37.2 1.3 slice_bitcast_fusion
  38.5 0.8 fusion.62
  39.3 0.8 broadcast_subtract_fusion
  40.1 0.8 reduce-scatter.13.cloned.1.call-done
  40.9 22.4 %reduce-scatter.15.cloned.1.call-done = f32[64,512]{1,0:T(8,128)} async-done(((f32[256,512]{1,0:T(8,128)}), f32[64,512]{1,0:T(8,128)}) %reduce-scatter.15.cloned.1.call-update) | async-done | bytes 131088 | tf_op jit(solution)/shard_map/reduce_scatter | solution.py:65
  63.4 22.4 %reduce-scatter.17.cloned.1.call-done = f32[64,512]{1,0:T(8,128)} async-done(((f32[256,512]{1,0:T(8,128)}), f32[64,512]{1,0:T(8,128)}) %reduce-scatter.17.cloned.1.call-update) | async-done | bytes 131088 | tf_op jit(solution)/shard_map/reduce_scatter | solution.py:65
  85.8 22.2 %reduce-scatter.11.cloned.1.call-done = f32[64,512]{1,0:T(8,128)} async-done(((f32[256,512]{1,0:T(8,128)}), f32[64,512]{1,0:T(8,128)}) %reduce-scatter.11.cloned.1.call-update) | async-done | bytes 131088 | tf_op jit(solution)/shard_map/reduce_scatter | solution.py:65
  108.0 1.2 multiply_add_fusion.3
  109.5 0.7 reshape.56
  110.2 0.7 reshape.61
  110.9 22.7 %fusion.4 = f32[64,4,1,128]{3,2,1,0:T(1,128)S(1)} fusion(f32[64,4,128,1]{2,3,1,0:T(1,128)} %bitcast.79, f32[2,64,4,128,128]{4,3,2,1,0:T(8,128)} %param.13, f32[64,4,128]{2,1,0:T(4,128)S(1)} %mul.316, f32[64,4,128]{2,1,0:T(4,128)S(1)} %mul.313, f32[64,4,128]{2,1,0:T(4,128)S(1)} %mul.309), kind=kOutput, calls=%fused_computation.6 | convolution fusion | flops 62914560 | bytes 17432576 | tf_op jit(solution)/shard_map/bhk,bhkv->bhv/dot_general | solution.py:22
  133.6 0.1 multiply_reduce_fusion.1
  133.8 0.1 fusion.61
  134.0 13.8 %all_gather.13 = bf16[256,512]{1,0:T(8,128)(2,1)S(1)} all-gather(bf16[64,512]{1,0:T(8,128)(2,1)S(1)} %bitcast.74), channel_id=1, replica_groups=mesh['grp'=2,'tp'=4,'dp'=4] {'dp'}, dimensions={0}, use_global_device_ids=true | all-gather | bytes 327680 | tf_op jit(solution)/shard_map/all_gather | solution.py:81
  147.8 2.1 fusion.30
  150.0 19.9 %reduce-scatter.19.cloned.1.call-done = f32[64,512]{1,0:T(8,128)} async-done(((f32[256,512]{1,0:T(8,128)}), f32[64,512]{1,0:T(8,128)}) %reduce-scatter.19.cloned.1.call-update) | async-done | bytes 131088 | tf_op jit(solution)/shard_map/reduce_scatter | solution.py:83
  169.9 0.9 add_convert_fusion
  170.9 5.8 %all_gather.14 = bf16[256,512]{1,0:T(8,128)(2,1)S(1)} all-gather(bf16[64,512]{1,0:T(8,128)(2,1)S(1)} %add_convert_fusion), channel_id=1, replica_groups=mesh['grp'=2,'tp'=4,'dp'=4] {'tp'}, dimensions={0}, use_global_device_ids=true | all-gather | bytes 327680 | tf_op jit(solution)/shard_map/all_gather | solution.py:51
  176.7 1.1 fusion.26
  177.8 1.1 fusion.24
  179.0 1.1 fusion.22
  180.2 2.2 fusion.28
  182.4 0.1 fusion.18
  182.6 11.7 %psum.15 = f32[256]{0:T(256)S(1)} all-reduce(f32[256]{0:T(256)S(1)} %fusion.18), channel_id=1, replica_groups=mesh['grp'=2,'tp'=4,'dp'=4] {'dp'}, use_global_device_ids=true, to_apply=%region_9.10 | all-reduce | flops 256 | bytes 2048 | tf_op jit(solution)/shard_map/psum | solution.py:54
  194.3 0.1 add_rsqrt_fusion.2
  194.4 5.5 %reduce-scatter.23.cloned.1.call-done = f32[64,512]{1,0:T(8,128)} async-done(((f32[256,512]{1,0:T(8,128)}), f32[64,512]{1,0:T(8,128)}) %reduce-scatter.23.cloned.1.call-update) | async-done | bytes 131088 | tf_op jit(solution)/shard_map/reduce_scatter | solution.py:65
  199.9 22.4 %reduce-scatter.25.cloned.1.call-done = f32[64,512]{1,0:T(8,128)} async-done(((f32[256,512]{1,0:T(8,128)}), f32[64,512]{1,0:T(8,128)}) %reduce-scatter.25.cloned.1.call-update) | async-done | bytes 131088 | tf_op jit(solution)/shard_map/reduce_scatter | solution.py:65
  222.3 22.4 %reduce-scatter.27.cloned.1.call-done = f32[64,512]{1,0:T(8,128)} async-done(((f32[256,512]{1,0:T(8,128)}), f32[64,512]{1,0:T(8,128)}) %reduce-scatter.27.cloned.1.call-update) | async-done | bytes 131088 | tf_op jit(solution)/shard_map/reduce_scatter | solution.py:65
  244.7 22.4 %reduce-scatter.21.cloned.1.call-done = f32[64,512]{1,0:T(8,128)} async-done(((f32[256,512]{1,0:T(8,128)}), f32[64,512]{1,0:T(8,128)}) %reduce-scatter.21.cloned.1.call-update) | async-done | bytes 131088 | tf_op jit(solution)/shard_map/reduce_scatter | solution.py:65
  267.1 1.2 multiply_add_fusion.2
  268.6 23.2 %multiply_add_fusion.1 = (f32[1,64,4,128,128]{4,3,2,1,0:T(8,128)}, f32[1,64,4,128,128]{4,3,2,1,0:T(8,128)}) fusion(f32[2,64,4,128,128]{4,3,2,1,0:T(8,128)} %param.13, f32[64,4,128]{2,1,0:T(4,128)} %copy-done.6, f32[64,4,128]{2,1,0:T(4,128)} %copy-done.5, f32[64,4,128]{2,1,0:T(4,128)} %copy-done.4, f32[64,4,128]{2,1,0:T(4,128)S(1)} %mul.349, ...), kind=kLoop, calls=%fused_computation.8 | loop fusion | flops 25165824 | bytes 67895296 | tf_op jit(solution)/shard_map/add | solution.py:21
  291.8 22.6 %fusion.1 = f32[64,4,1,128]{3,2,1,0:T(1,128)S(1)} fusion(f32[64,4,128,1]{2,3,1,0:T(1,128)S(1)} %bitcast.78, f32[2,64,4,128,128]{4,3,2,1,0:T(8,128)} %param.13, f32[64,4,128]{2,1,0:T(4,128)S(1)} %mul.349, f32[64,4,128]{2,1,0:T(4,128)S(1)} %mul.346, f32[64,4,128]{2,1,0:T(4,128)S(1)} %mul.342), kind=kOutput, calls=%fused_computation.3 | convolution fusion | flops 62914560 | bytes 17432576 | tf_op jit(solution)/shard_map/bhk,bhkv->bhv/dot_general | solution.py:22
  314.4 0.1 multiply_reduce_fusion
  314.6 0.1 fusion.60
  314.8 13.8 %all_gather.15 = bf16[256,512]{1,0:T(8,128)(2,1)S(1)} all-gather(bf16[64,512]{1,0:T(8,128)(2,1)S(1)} %bitcast.75), channel_id=1, replica_groups=mesh['grp'=2,'tp'=4,'dp'=4] {'dp'}, dimensions={0}, use_global_device_ids=true | all-gather | bytes 327680 | tf_op jit(solution)/shard_map/all_gather | solution.py:81
  328.6 1.1 fusion.20
  329.7 23.4 %pad_maximum_fusion = f32[2,64,4,128,128]{4,3,2,1,0:T(8,128)} fusion(f32[1,64,4,128,128]{4,3,2,1,0:T(8,128)} %get-tuple-element.7, f32[1,64,4,128,128]{4,3,2,1,0:T(8,128)} %get-tuple-element.6), kind=kLoop, calls=%fused_computation | loop fusion | flops 8388608 | bytes 67108864 | tf_op jit(solution)/shard_map/stack | solution.py:93
  353.1 1.6 convert_add_fusion
  (55 shorter events, 1.1 us)
Async XLA Ops:
  7.2 33.7 %reduce-scatter.13.cloned.1.call-start = ((), (), s32[]{:S(2)}) async-start(), calls=%async_computation.11 | async-start | bytes 655360 | tf_op jit(solution)/shard_map/reduce_scatter | solution.py:65
  17.6 45.8 %reduce-scatter.15.cloned.1.call-start = ((), (), s32[]{:S(2)}) async-start(), calls=%async_computation.12 | async-start | bytes 655360 | tf_op jit(solution)/shard_map/reduce_scatter | solution.py:65
  19.8 66.0 %reduce-scatter.17.cloned.1.call-start = ((), (), s32[]{:S(2)}) async-start(), calls=%async_computation.13 | async-start | bytes 655360 | tf_op jit(solution)/shard_map/reduce_scatter | solution.py:65
  22.0 86.0 %reduce-scatter.11.cloned.1.call-start = ((), (), s32[]{:S(2)}) async-start(), calls=%async_computation.10 | async-start | bytes 655360 | tf_op jit(solution)/shard_map/reduce_scatter | solution.py:65
  24.3 145.7 %reduce-scatter.19.cloned.1.call-start = ((), (), s32[]{:S(2)}) async-start(), calls=%async_computation.14 | async-start | bytes 655360 | tf_op jit(solution)/shard_map/reduce_scatter | solution.py:83
  37.2 73.7 %copy-start.8 = (f32[64]{0:T(128)}, f32[64]{0:T(128)S(1)}, u32[]{:S(2)}) copy-start(f32[64]{0:T(128)S(1)} %multiply_log_fusion) | copy-start | bytes 772
  109.3 24.6 %copy-start.4 = (f32[64,4,128]{2,1,0:T(4,128)}, f32[64,4,128]{2,1,0:T(4,128)S(1)}, u32[]{:S(2)}) copy-start(f32[64,4,128]{2,1,0:T(4,128)S(1)} %mul.309) | copy-start | bytes 393220
  109.4 24.6 %copy-start.5 = (f32[64,4,128]{2,1,0:T(4,128)}, f32[64,4,128]{2,1,0:T(4,128)S(1)}, u32[]{:S(2)}) copy-start(f32[64,4,128]{2,1,0:T(4,128)S(1)} %mul.313) | copy-start | bytes 393220
  109.5 40.5 %copy-start.6 = (f32[64,4,128]{2,1,0:T(4,128)}, f32[64,4,128]{2,1,0:T(4,128)S(1)}, u32[]{:S(2)}) copy-start(f32[64,4,128]{2,1,0:T(4,128)S(1)} %mul.316) | copy-start | bytes 393220
  110.9 22.9 %copy-start.7 = (f32[64,4,128]{2,1,0:T(4,128)S(1)}, f32[64,4,128]{2,1,0:T(4,128)}, u32[]{:S(2)}) copy-start(f32[64,4,128]{2,1,0:T(4,128)} %reshape.56) | copy-start | bytes 393220
  110.9 22.9 %copy-start.10 = (f32[128]{0:T(128)S(1)}, f32[128]{0:T(128)}, u32[]{:S(2)}) copy-start(f32[128]{0:T(128)} %get-tuple-element.19) | copy-start | bytes 1540
  110.9 65.8 %copy-start = (bf16[2,512,512]{2,1,0:T(8,128)(2,1)S(1)}, bf16[2,512,512]{2,1,0:T(8,128)(2,1)}, u32[]{:S(2)}) copy-start(bf16[2,512,512]{2,1,0:T(8,128)(2,1)} %param.17) | copy-start | bytes 3145732
  110.9 66.9 %copy-start.1 = (bf16[2,512,512]{2,1,0:T(8,128)(2,1)S(1)}, bf16[2,512,512]{2,1,0:T(8,128)(2,1)}, u32[]{:S(2)}) copy-start(bf16[2,512,512]{2,1,0:T(8,128)(2,1)} %param.18) | copy-start | bytes 3145732
  110.9 68.1 %copy-start.2 = (bf16[2,512,512]{2,1,0:T(8,128)(2,1)S(1)}, bf16[2,512,512]{2,1,0:T(8,128)(2,1)}, u32[]{:S(2)}) copy-start(bf16[2,512,512]{2,1,0:T(8,128)(2,1)} %param.19) | copy-start | bytes 3145732
  150.0 49.9 %reduce-scatter.23.cloned.1.call-start = ((), (), s32[]{:S(2)}) async-start(), calls=%async_computation.16 | async-start | bytes 655360 | tf_op jit(solution)/shard_map/reduce_scatter | solution.py:65
  177.8 44.5 %reduce-scatter.25.cloned.1.call-start = ((), (), s32[]{:S(2)}) async-start(), calls=%async_computation.17 | async-start | bytes 655360 | tf_op jit(solution)/shard_map/reduce_scatter | solution.py:65
  178.9 65.7 %reduce-scatter.27.cloned.1.call-start = ((), (), s32[]{:S(2)}) async-start(), calls=%async_computation.18 | async-start | bytes 655360 | tf_op jit(solution)/shard_map/reduce_scatter | solution.py:65
  180.1 86.9 %reduce-scatter.21.cloned.1.call-start = ((), (), s32[]{:S(2)}) async-start(), calls=%async_computation.15 | async-start | bytes 655360 | tf_op jit(solution)/shard_map/reduce_scatter | solution.py:65
  182.4 170.8 %reduce-scatter.29.cloned.1.call-start = ((), (), s32[]{:S(2)}) async-start(), calls=%async_computation.19 | async-start | bytes 655360 | tf_op jit(solution)/shard_map/reduce_scatter | solution.py:83
  291.8 22.8 %copy-start.9 = (f32[128]{0:T(128)S(1)}, f32[128]{0:T(128)}, u32[]{:S(2)}) copy-start(f32[128]{0:T(128)} %get-tuple-element.18) | copy-start | bytes 1540
  291.8 36.8 %copy-start.3 = (bf16[2,512,512]{2,1,0:T(8,128)(2,1)S(1)}, bf16[2,512,512]{2,1,0:T(8,128)(2,1)}, u32[]{:S(2)}) copy-start(bf16[2,512,512]{2,1,0:T(8,128)(2,1)} %param.20) | copy-start | bytes 3145732
Sparse Core Ops, SparseCore 0:
  17.7 23.1 reduce-scatter.12
  43.2 20.1 reduce-scatter.14
  65.6 20.1 reduce-scatter.16
  87.9 20.0 reduce-scatter.10
  150.1 19.8 reduce-scatter.18
  177.9 21.9 reduce-scatter.22
  202.2 20.0 reduce-scatter.24
  224.6 20.0 reduce-scatter.26
  247.0 20.0 reduce-scatter.20
  329.8 19.8 reduce-scatter.28
where the time goes:
time: 362 us
  waiting for transfers between devices  161 us (44%)
  blocking collectives  64.5 us (18%)
  matrix products  62.6 us (17%)
  other arithmetic  54.8 us (15%)
  between operations  14.5 us (4%)
  local copies, waits for them, and re-layouts  3.97 us (1%)
    reduce_scatter x8, waiting for transfers between devices, shards(): sums = lax.psum_scatter(terms, 'dp', scatter_dimension=0, tiled=True)  141 us
    dot_general x2, matrix products, advance(): jnp.einsum('bhk,bhkv->bhv', query.reshape(count, heads, size), updated, p...  45.3 us
    all_gather x2, blocking collectives, shards(): gathered = lax.all_gather(normed, 'dp', axis=0, tiled=True)  27.6 us
    psum x2, blocking collectives, shards(): squares_all = lax.psum(partial_sq, 'dp')  23.7 us
    another operation x1, other arithmetic, shards(): return (result, jnp.stack(states))  23.4 us
    add x1, other arithmetic, advance(): updated = forget[..., None] * prior + key[..., None] * values[:, :, None, :]  23.2 us
    reduce_scatter x2, waiting for transfers between devices, shards(): lax.psum_scatter(jnp.dot(gathered, out_weight, preferred_element_type=jnp...  19.9 us
    dot_general x8, matrix products, shards(): jnp.dot(gained, weight[block], preferred_element_type=jnp.float32)  14.1 us
  transfers between devices with their start and end apart: 10, of which 9 were waited for; matrix products, arithmetic and copies ran while one was open for 11% of the time, Pallas kernels for 0%

commit v1 on v0

--- a/solution.py
+++ b/solution.py
@@ -78,7 +78,10 @@
             head_gain[block],
         )
         states.append(updated)
-        gathered = lax.all_gather(normed, "dp", axis=0, tiled=True)
+        n_dev = lax.axis_size("dp")
+        pieces = jnp.stack([normed for _ in range(n_dev)])
+        pieces = lax.all_to_all(pieces, "dp", split_axis=0, concat_axis=0)
+        gathered = jnp.concatenate(pieces, axis=0)
         out_weight = w_out[block]
         branch = lax.psum_scatter(
             jnp.dot(gathered, out_weight, preferred_element_type=jnp.float32),

time: 362 us -> 349 us (0.964)
  blocking collectives: 64.5 us -> 47.1 us
    all_gather x2 -> x0, blocking collectives: 27.6 us -> none  [shards(): gathered = lax.all_gather(normed, 'dp', axis=0, tiled=True)]
    all_to_all x0 -> x1, blocking collectives: none -> 10.1 us  [shards(): pieces = lax.all_to_all(pieces, 'dp', split_axis=0, concat_axis=0)]
  transfers between devices with their start and end apart: 10 -> 11, of which waited for: 9 -> 9; matrix products, arithmetic and copies ran while one was open for 11% -> 18% of each run, Pallas kernels for 0% -> 0%
where the time goes in v1:
time: 349 us
  waiting for transfers between devices  162 us (46%)
  matrix products  62.5 us (18%)
  other arithmetic  54.6 us (16%)
  blocking collectives  47.1 us (13%)
  between operations  14.5 us (4%)
  local copies, waits for them, and re-layouts  4.64 us (1%)
  starting transfers between devices  3.82 us (1%)
    reduce_scatter x8, waiting for transfers between devices, shards(): sums = lax.psum_scatter(terms, 'dp', scatter_dimension=0, tiled=True)  141 us
    dot_general x2, matrix products, advance(): jnp.einsum('bhk,bhkv->bhv', query.reshape(count, heads, size), updated, p...  45.2 us
    psum x2, blocking collectives, shards(): squares_all = lax.psum(partial_sq, 'dp')  23.7 us
    another operation x1, other arithmetic, shards(): return (result, jnp.stack(states))  23.4 us
    add x1, other arithmetic, advance(): updated = forget[..., None] * prior + key[..., None] * values[:, :, None, :]  23 us
    reduce_scatter x2, waiting for transfers between devices, shards(): lax.psum_scatter(jnp.dot(gathered, out_weight, preferred_element_type=jnp...  20.6 us
    dot_general x8, matrix products, shards(): jnp.dot(gained, weight[block], preferred_element_type=jnp.float32)  14 us
    all_gather x2, blocking collectives, shards(): whole = lax.all_gather(current, 'tp', axis=0, tiled=True)  13.2 us
  transfers between devices with their start and end apart: 11, of which 9 were waited for; matrix products, arithmetic and copies ran while one was open for 18% of the time, Pallas kernels for 0%

profile of v1, /device:TPU:0, one launch (start us, length us, event | category | flops | bytes accessed | tf_op | source)
XLA Modules:
  0.0 348.6 jit_solution(3910906539653043264)
XLA Ops:
  7.2 0.8 slice_convert_fusion
  8.0 7.4 %all_gather.6 = bf16[256,512]{1,0:T(8,128)(2,1)S(1)} all-gather(bf16[64,512]{1,0:T(8,128)(2,1)} %param.12), channel_id=1, replica_groups=mesh['grp'=2,'tp'=4,'dp'=4] {'tp'}, dimensions={0}, use_global_device_ids=true | all-gather | bytes 327680 | tf_op jit(solution)/shard_map/all_gather | solution.py:51
  15.4 2.1 fusion.36
  17.6 2.1 fusion.34
  19.8 2.1 fusion.32
  22.1 2.2 fusion.38
  24.3 0.1 fusion.16
  24.4 12.0 %psum.14 = f32[256]{0:T(256)S(1)} all-reduce(f32[256]{0:T(256)S(1)} %fusion.16), channel_id=1, replica_groups=mesh['grp'=2,'tp'=4,'dp'=4] {'dp'}, use_global_device_ids=true, to_apply=%region_1.0 | all-reduce | flops 256 | bytes 2048 | tf_op jit(solution)/shard_map/psum | solution.py:54
  36.4 0.1 add_rsqrt_fusion.3
  36.5 0.7 multiply_log_fusion
  37.2 1.3 slice_bitcast_fusion
  38.5 0.8 fusion.62
  39.2 0.8 broadcast_subtract_fusion
  40.0 0.9 reduce-scatter.13.cloned.1.call-done
  40.9 22.4 %reduce-scatter.15.cloned.1.call-done = f32[64,512]{1,0:T(8,128)} async-done(((f32[256,512]{1,0:T(8,128)}), f32[64,512]{1,0:T(8,128)}) %reduce-scatter.15.cloned.1.call-update) | async-done | bytes 131088 | tf_op jit(solution)/shard_map/reduce_scatter | solution.py:65
  63.4 22.4 %reduce-scatter.17.cloned.1.call-done = f32[64,512]{1,0:T(8,128)} async-done(((f32[256,512]{1,0:T(8,128)}), f32[64,512]{1,0:T(8,128)}) %reduce-scatter.17.cloned.1.call-update) | async-done | bytes 131088 | tf_op jit(solution)/shard_map/reduce_scatter | solution.py:65
  85.8 22.2 %reduce-scatter.11.cloned.1.call-done = f32[64,512]{1,0:T(8,128)} async-done(((f32[256,512]{1,0:T(8,128)}), f32[64,512]{1,0:T(8,128)}) %reduce-scatter.11.cloned.1.call-update) | async-done | bytes 131088 | tf_op jit(solution)/shard_map/reduce_scatter | solution.py:65
  108.0 1.2 multiply_add_fusion.3
  109.5 0.7 reshape.68
  110.2 0.7 reshape.75
  110.9 22.7 %fusion.4 = f32[64,4,1,128]{3,2,1,0:T(1,128)S(1)} fusion(f32[64,4,128,1]{2,3,1,0:T(1,128)} %bitcast.82, f32[2,64,4,128,128]{4,3,2,1,0:T(8,128)} %param.13, f32[64,4,128]{2,1,0:T(4,128)S(1)} %mul.316, f32[64,4,128]{2,1,0:T(4,128)S(1)} %mul.313, f32[64,4,128]{2,1,0:T(4,128)S(1)} %mul.309), kind=kOutput, calls=%fused_computation.6 | convolution fusion | flops 62914560 | bytes 17432576 | tf_op jit(solution)/shard_map/bhk,bhkv->bhv/dot_general | solution.py:22
  133.6 0.1 multiply_reduce_fusion.1
  133.8 0.1 fusion.61
  134.0 10.1 %all_to_all.10 = bf16[4,64,512]{2,1,0:T(8,128)(2,1)S(1)} all-to-all(bf16[4,64,512]{2,1,0:T(8,128)(2,1)S(1)} %stack.6), channel_id=1, replica_groups=mesh['grp'=2,'tp'=4,'dp'=4] {'dp'}, dimensions={0} | all-to-all | bytes 524288 | tf_op jit(solution)/shard_map/all_to_all | solution.py:83
  144.1 2.1 fusion.30
  146.4 20.6 %reduce-scatter.19.cloned.1.call-done = f32[64,512]{1,0:T(8,128)} async-done(((f32[256,512]{1,0:T(8,128)}), f32[64,512]{1,0:T(8,128)}) %reduce-scatter.19.cloned.1.call-update) | async-done | bytes 131088 | tf_op jit(solution)/shard_map/reduce_scatter | solution.py:86
  166.9 0.9 add_convert_fusion
  167.9 5.8 %all_gather.7 = bf16[256,512]{1,0:T(8,128)(2,1)S(1)} all-gather(bf16[64,512]{1,0:T(8,128)(2,1)S(1)} %add_convert_fusion), channel_id=1, replica_groups=mesh['grp'=2,'tp'=4,'dp'=4] {'tp'}, dimensions={0}, use_global_device_ids=true | all-gather | bytes 327680 | tf_op jit(solution)/shard_map/all_gather | solution.py:51
  173.6 1.1 fusion.26
  174.8 1.1 fusion.24
  176.0 1.1 fusion.22
  177.2 2.2 fusion.28
  179.4 0.1 fusion.18
  179.5 11.7 %psum.15 = f32[256]{0:T(256)S(1)} all-reduce(f32[256]{0:T(256)S(1)} %fusion.18), channel_id=1, replica_groups=mesh['grp'=2,'tp'=4,'dp'=4] {'dp'}, use_global_device_ids=true, to_apply=%region_9.10 | all-reduce | flops 256 | bytes 2048 | tf_op jit(solution)/shard_map/psum | solution.py:54
  191.3 5.6 %reduce-scatter.23.cloned.1.call-done = f32[64,512]{1,0:T(8,128)} async-done(((f32[256,512]{1,0:T(8,128)}), f32[64,512]{1,0:T(8,128)}) %reduce-scatter.23.cloned.1.call-update) | async-done | bytes 131088 | tf_op jit(solution)/shard_map/reduce_scatter | solution.py:65
  196.9 22.4 %reduce-scatter.25.cloned.1.call-done = f32[64,512]{1,0:T(8,128)} async-done(((f32[256,512]{1,0:T(8,128)}), f32[64,512]{1,0:T(8,128)}) %reduce-scatter.25.cloned.1.call-update) | async-done | bytes 131088 | tf_op jit(solution)/shard_map/reduce_scatter | solution.py:65
  219.2 22.4 %reduce-scatter.27.cloned.1.call-done = f32[64,512]{1,0:T(8,128)} async-done(((f32[256,512]{1,0:T(8,128)}), f32[64,512]{1,0:T(8,128)}) %reduce-scatter.27.cloned.1.call-update) | async-done | bytes 131088 | tf_op jit(solution)/shard_map/reduce_scatter | solution.py:65
  241.6 22.4 %reduce-scatter.21.cloned.1.call-done = f32[64,512]{1,0:T(8,128)} async-done(((f32[256,512]{1,0:T(8,128)}), f32[64,512]{1,0:T(8,128)}) %reduce-scatter.21.cloned.1.call-update) | async-done | bytes 131088 | tf_op jit(solution)/shard_map/reduce_scatter | solution.py:65
  264.1 1.3 multiply_add_fusion.2
  265.6 22.5 %fusion.1 = f32[64,4,1,128]{3,2,1,0:T(1,128)S(1)} fusion(f32[64,4,128,1]{2,3,1,0:T(1,128)S(1)} %bitcast.83, f32[2,64,4,128,128]{4,3,2,1,0:T(8,128)} %param.13, f32[64,4,128]{2,1,0:T(4,128)S(1)} %mul.349, f32[64,4,128]{2,1,0:T(4,128)S(1)} %mul.346, f32[64,4,128]{2,1,0:T(4,128)S(1)} %mul.342), kind=kOutput, calls=%fused_computation.3 | convolution fusion | flops 62914560 | bytes 17432576 | tf_op jit(solution)/shard_map/bhk,bhkv->bhv/dot_general | solution.py:22
  288.2 0.1 multiply_reduce_fusion
  288.3 0.1 fusion.60
  288.5 0.7 stack.7
  289.2 3.4 all-to-all-start.1
  292.7 23.0 %multiply_add_fusion.1 = (f32[1,64,4,128,128]{4,3,2,1,0:T(8,128)}, f32[1,64,4,128,128]{4,3,2,1,0:T(8,128)}) fusion(f32[2,64,4,128,128]{4,3,2,1,0:T(8,128)} %param.13, f32[64,4,128]{2,1,0:T(4,128)S(1)} %copy-done.9, f32[64,4,128]{2,1,0:T(4,128)S(1)} %copy-done.7, f32[64,4,128]{2,1,0:T(4,128)S(1)} %copy-done.5, f32[64,4,128]{2,1,0:T(4,128)S(1)} %mul.349, ...), kind=kLoop, calls=%fused_computation.8 | loop fusion | flops 25165824 | bytes 67895296 | tf_op jit(solution)/shard_map/add | solution.py:21
  315.7 1.1 fusion.20
  316.8 23.4 %pad_maximum_fusion = f32[2,64,4,128,128]{4,3,2,1,0:T(8,128)} fusion(f32[1,64,4,128,128]{4,3,2,1,0:T(8,128)} %get-tuple-element.7, f32[1,64,4,128,128]{4,3,2,1,0:T(8,128)} %get-tuple-element.6), kind=kLoop, calls=%fused_computation | loop fusion | flops 8388608 | bytes 67108864 | tf_op jit(solution)/shard_map/stack | solution.py:96
  340.2 1.6 convert_add_fusion
  (64 shorter events, 1.2 us)
Async XLA Ops:
  7.2 33.7 %reduce-scatter.13.cloned.1.call-start = ((), (), s32[]{:S(2)}) async-start(), calls=%async_computation.13 | async-start | bytes 655360 | tf_op jit(solution)/shard_map/reduce_scatter | solution.py:65
  17.6 45.8 %reduce-scatter.15.cloned.1.call-start = ((), (), s32[]{:S(2)}) async-start(), calls=%async_computation.14 | async-start | bytes 655360 | tf_op jit(solution)/shard_map/reduce_scatter | solution.py:65
  19.8 66.0 %reduce-scatter.17.cloned.1.call-start = ((), (), s32[]{:S(2)}) async-start(), calls=%async_computation.15 | async-start | bytes 655360 | tf_op jit(solution)/shard_map/reduce_scatter | solution.py:65
  22.0 86.0 %reduce-scatter.11.cloned.1.call-start = ((), (), s32[]{:S(2)}) async-start(), calls=%async_computation.12 | async-start | bytes 655360 | tf_op jit(solution)/shard_map/reduce_scatter | solution.py:65
  24.2 142.7 %reduce-scatter.19.cloned.1.call-start = ((), (), s32[]{:S(2)}) async-start(), calls=%async_computation.16 | async-start | bytes 655360 | tf_op jit(solution)/shard_map/reduce_scatter | solution.py:86
  37.2 73.7 %copy-start.11 = (f32[64]{0:T(128)}, f32[64]{0:T(128)S(1)}, u32[]{:S(2)}) copy-start(f32[64]{0:T(128)S(1)} %multiply_log_fusion) | copy-start | bytes 772
  109.3 24.6 %copy-start.4 = (f32[64,4,128]{2,1,0:T(4,128)}, f32[64,4,128]{2,1,0:T(4,128)S(1)}, u32[]{:S(2)}) copy-start(f32[64,4,128]{2,1,0:T(4,128)S(1)} %mul.309) | copy-start | bytes 393220
  109.4 24.6 %copy-start.6 = (f32[64,4,128]{2,1,0:T(4,128)}, f32[64,4,128]{2,1,0:T(4,128)S(1)}, u32[]{:S(2)}) copy-start(f32[64,4,128]{2,1,0:T(4,128)S(1)} %mul.313) | copy-start | bytes 393220
  109.4 36.9 %copy-start.8 = (f32[64,4,128]{2,1,0:T(4,128)}, f32[64,4,128]{2,1,0:T(4,128)S(1)}, u32[]{:S(2)}) copy-start(f32[64,4,128]{2,1,0:T(4,128)S(1)} %mul.316) | copy-start | bytes 393220
  110.9 22.9 %copy-start.10 = (f32[64,4,128]{2,1,0:T(4,128)S(1)}, f32[64,4,128]{2,1,0:T(4,128)}, u32[]{:S(2)}) copy-start(f32[64,4,128]{2,1,0:T(4,128)} %reshape.68) | copy-start | bytes 393220
  110.9 22.9 %copy-start.13 = (f32[128]{0:T(128)S(1)}, f32[128]{0:T(128)}, u32[]{:S(2)}) copy-start(f32[128]{0:T(128)} %get-tuple-element.19) | copy-start | bytes 1540
  110.9 62.8 %copy-start = (bf16[2,512,512]{2,1,0:T(8,128)(2,1)S(1)}, bf16[2,512,512]{2,1,0:T(8,128)(2,1)}, u32[]{:S(2)}) copy-start(bf16[2,512,512]{2,1,0:T(8,128)(2,1)} %param.17) | copy-start | bytes 3145732
  110.9 64.0 %copy-start.1 = (bf16[2,512,512]{2,1,0:T(8,128)(2,1)S(1)}, bf16[2,512,512]{2,1,0:T(8,128)(2,1)}, u32[]{:S(2)}) copy-start(bf16[2,512,512]{2,1,0:T(8,128)(2,1)} %param.18) | copy-start | bytes 3145732
  110.9 65.1 %copy-start.2 = (bf16[2,512,512]{2,1,0:T(8,128)(2,1)S(1)}, bf16[2,512,512]{2,1,0:T(8,128)(2,1)}, u32[]{:S(2)}) copy-start(bf16[2,512,512]{2,1,0:T(8,128)(2,1)} %param.19) | copy-start | bytes 3145732
  146.3 50.6 %reduce-scatter.23.cloned.1.call-start = ((), (), s32[]{:S(2)}) async-start(), calls=%async_computation.18 | async-start | bytes 655360 | tf_op jit(solution)/shard_map/reduce_scatter | solution.py:65
  174.8 44.5 %reduce-scatter.25.cloned.1.call-start = ((), (), s32[]{:S(2)}) async-start(), calls=%async_computation.19 | async-start | bytes 655360 | tf_op jit(solution)/shard_map/reduce_scatter | solution.py:65
  175.9 65.7 %reduce-scatter.27.cloned.1.call-start = ((), (), s32[]{:S(2)}) async-start(), calls=%async_computation.20 | async-start | bytes 655360 | tf_op jit(solution)/shard_map/reduce_scatter | solution.py:65
  177.1 86.9 %reduce-scatter.21.cloned.1.call-start = ((), (), s32[]{:S(2)}) async-start(), calls=%async_computation.17 | async-start | bytes 655360 | tf_op jit(solution)/shard_map/reduce_scatter | solution.py:65
  179.3 109.0 %copy-start.12 = (f32[128]{0:T(128)S(1)}, f32[128]{0:T(128)}, u32[]{:S(2)}) copy-start(f32[128]{0:T(128)} %get-tuple-element.18) | copy-start | bytes 1540
  264.0 28.7 %copy-start.5 = (f32[64,4,128]{2,1,0:T(4,128)S(1)}, f32[64,4,128]{2,1,0:T(4,128)}, u32[]{:S(2)}) copy-start(f32[64,4,128]{2,1,0:T(4,128)} %copy-done.4) | copy-start | bytes 393220
  264.0 28.7 %copy-start.7 = (f32[64,4,128]{2,1,0:T(4,128)S(1)}, f32[64,4,128]{2,1,0:T(4,128)}, u32[]{:S(2)}) copy-start(f32[64,4,128]{2,1,0:T(4,128)} %copy-done.6) | copy-start | bytes 393220
  264.1 28.7 %copy-start.9 = (f32[64,4,128]{2,1,0:T(4,128)S(1)}, f32[64,4,128]{2,1,0:T(4,128)}, u32[]{:S(2)}) copy-start(f32[64,4,128]{2,1,0:T(4,128)} %copy-done.8) | copy-start | bytes 393220
  289.2 26.5 %all-to-all-start.1 = ((bf16[4,64,512]{2,1,0:T(8,128)(2,1)}), bf16[4,64,512]{2,1,0:T(8,128)(2,1)S(1)}, u32[]{:S(2)}, u32[]{:S(2)}) async-start(bf16[4,64,512]{2,1,0:T(8,128)(2,1)} %stack.7), calls=%async_computation.10 | async-start | bytes 524288 | tf_op jit(solution)/shard_map/all_to_all | solution.py:83
  292.6 23.1 %copy-start.3 = (bf16[2,512,512]{2,1,0:T(8,128)(2,1)S(1)}, bf16[2,512,512]{2,1,0:T(8,128)(2,1)}, u32[]{:S(2)}) copy-start(bf16[2,512,512]{2,1,0:T(8,128)(2,1)} %param.20) | copy-start | bytes 3145732
  292.7 47.6 %reduce-scatter.29.cloned.1.call-start = ((), (), s32[]{:S(2)}) async-start(), calls=%async_computation.21 | async-start | bytes 655360 | tf_op jit(solution)/shard_map/reduce_scatter | solution.py:86
Sparse Core Ops, SparseCore 0:
  17.7 23.1 reduce-scatter.12
  43.2 20.1 reduce-scatter.14
  65.6 20.1 reduce-scatter.16
  87.9 20.0 reduce-scatter.10
  146.4 20.4 reduce-scatter.18
  174.9 21.9 reduce-scatter.22
  199.2 20.0 reduce-scatter.24
  221.5 20.0 reduce-scatter.26
  243.9 20.0 reduce-scatter.20
  317.0 22.8 reduce-scatter.28
